TPU v7x, 32 devices: a whole 2x2x4 slice. The times are simulated.
32 devices in a mesh: grp: 2 (over y), sp: 4 (over z), tp: 4 (over x, core).
Axes of the slice: x: 2, y: 2, z: 4, core: 2. Of those that a mesh axis runs over, the one named last changes fastest.
Arguments:
- stream: bfloat16 [2048, 2048], P(('grp', 'sp')), parts along dimension 0, may hold values from -6 to 6
- doc_ids: int32 [2048], P(('grp', 'sp')), parts along dimension 0, may hold values from 0 to 1, never falling along the last dimension, each value on 1 to 768 neighbouring positions
- norm_gain: float32 [2, 2048], replicated, may hold values from 0.1 to 1.9
- query_weight: bfloat16 [2, 2048, 1024], P(None, 'sp', 'tp'), may hold values from -0.125 to 0.125
- key_weight: bfloat16 [2, 2048, 1024], P(None, 'sp', 'tp'), may hold values from -0.125 to 0.125
- value_weight: bfloat16 [2, 2048, 1024], P(None, 'sp', 'tp'), may hold values from -0.125 to 0.125
- out_weight: bfloat16 [2, 1024, 2048], P(None, 'sp', 'tp'), may hold values from -0.75 to 0.75
- query_gain: float32 [2, 64], replicated, may hold values from 0.1 to 1.9
- key_gain: float32 [2, 64], replicated, may hold values from 0.1 to 1.9
- rel_bias: float32 [16, 513], P('tp'), may hold values from -4 to 250
Outputs:
- encoded: bfloat16 [2048, 2048], P(('grp', 'sp')), parts along dimension 0
There are 2 independent parts, one for each index of `grp`. A program takes and returns all parts, laid end to end along the dimension named above; an argument that names none is the same for every part. Nothing has to cross between parts.
Inputs may be any that keep to these rules, and one draw needn't show every extreme that they name: doc_ids never fall along the sequence; each document has at most 768 positions.
All inputs are finite; a program needn't handle non-finite values.
Results may differ from a plain program's by a relative error of at most 0.011.
Values may be sent and summed in bfloat16 or wider, within the bound.
No kernel may reach another device: no remote copies, remote signals or barrier semaphores. Data moves between devices by JAX's collectives and lax.ppermute only.
A program may use at most 64 MiB of HBM per device.

v0:
```python
import jax
import jax.numpy as jnp
from jax import lax
from jax.sharding import PartitionSpec as P

SEG = 64
LEFT = 8
MAXREL = 256
LAYERS = 2
epsilon = 1e-06


def shifted(value, axis, steps):
    count = lax.axis_size(axis)
    initial, last = (max(0, -steps), min(count, count - steps))
    return lax.ppermute(value, axis, [(source, source + steps) for source in range(initial, last)])


def row_norm(values, gain):
    return values * lax.rsqrt(jnp.mean(values * values, axis=-1, keepdims=True) + epsilon) * gain


def bias_table(rel_bias):
    heads_here = rel_bias.shape[0]
    reach = LEFT * SEG
    width = (LEFT + 1) * SEG
    highest = reach + SEG - 1
    reversed_bias = rel_bias[:, ::-1]
    upper_fill = jnp.broadcast_to(rel_bias[:, -1:], (heads_here, highest - MAXREL))
    flat_row = jnp.concatenate([upper_fill, reversed_bias[:, : MAXREL + SEG]], axis=1)
    lines = [
        flat_row[:, SEG - 1 - position : SEG - 1 - position + width] for position in range(SEG)
    ]
    return jnp.stack(lines, axis=1)


def attend(query, ext_keys, ext_values, ext_docs, own_docs, offset, table):
    rows, heads_here, head_size = query.shape
    count = rows // SEG
    width = (LEFT + 1) * SEG
    blocks = query.reshape(count, SEG, heads_here, head_size)
    key_blocks = ext_keys.reshape(count + LEFT, SEG, heads_here, head_size)
    value_blocks = ext_values.reshape(count + LEFT, SEG, heads_here, head_size)
    doc_blocks = ext_docs.reshape(count + LEFT, SEG)
    score_parts = [
        jnp.einsum(
            "nqhd,nkhd->nhqk",
            blocks,
            key_blocks[earlier : earlier + count],
            preferred_element_type=jnp.float32,
        )
        for earlier in range(LEFT + 1)
    ]
    scores = jnp.concatenate(score_parts, axis=-1)
    scores = scores * head_size ** (-0.5) + table[None]
    doc_band = jnp.concatenate(
        [doc_blocks[earlier : earlier + count] for earlier in range(LEFT + 1)], axis=1
    )
    key_pos = (
        offset
        + SEG * jnp.arange(count, dtype=jnp.int32)[:, None]
        - LEFT * SEG
        + jnp.arange(width, dtype=jnp.int32)[None, :]
    )
    allowed = (key_pos >= 0)[:, None, None, :] & (
        doc_band[:, None, None, :] == own_docs.reshape(count, SEG)[:, None, :, None]
    )
    scores = jnp.where(allowed, scores, -1e30)
    peak = jnp.max(scores, axis=-1, keepdims=True)
    expo = jnp.exp(scores - peak)
    weights = (expo / jnp.sum(expo, axis=-1, keepdims=True)).astype(jnp.bfloat16)
    mixed = jnp.zeros((count, SEG, heads_here, head_size), jnp.float32)
    for earlier in range(LEFT + 1):
        part_weights = weights[..., earlier * SEG : (earlier + 1) * SEG]
        mixed = mixed + jnp.einsum(
            "nhqk,nkhd->nqhd",
            part_weights,
            value_blocks[earlier : earlier + count],
            preferred_element_type=jnp.float32,
        )
    return mixed.astype(jnp.bfloat16).reshape(rows, heads_here * head_size)


def on_device(
    stream,
    doc_ids,
    norm_gain,
    query_weight,
    key_weight,
    value_weight,
    out_weight,
    query_gain,
    key_gain,
    rel_bias,
):
    rows = stream.shape[0]
    heads_here = rel_bias.shape[0]
    head_size = query_gain.shape[1]
    local_width = heads_here * head_size
    reach = LEFT * SEG
    depth = -(-reach // rows)
    offset = lax.axis_index("sp") * rows
    col_width = out_weight.shape[2]
    col_start = lax.axis_index("tp") * col_width
    table = bias_table(rel_bias)
    x = stream
    for layer in range(LAYERS):
        widened = x.astype(jnp.float32)
        normed = row_norm(widened, norm_gain[layer]).astype(jnp.bfloat16)
        own_cols = normed
        q_raw = jnp.dot(
            own_cols,
            lax.all_gather(query_weight[layer], "sp", axis=0, tiled=True),
            preferred_element_type=jnp.float32,
        )
        k_raw = jnp.dot(
            normed,
            lax.all_gather(key_weight[layer], "sp", axis=0, tiled=True),
            preferred_element_type=jnp.float32,
        )
        v_raw = jnp.dot(
            normed,
            lax.all_gather(value_weight[layer], "sp", axis=0, tiled=True),
            preferred_element_type=jnp.float32,
        )
        query = row_norm(q_raw.reshape(rows, heads_here, head_size), query_gain[layer]).astype(
            jnp.bfloat16
        )
        keys = row_norm(
            k_raw.reshape(normed.shape[0], heads_here, head_size), key_gain[layer]
        ).astype(jnp.bfloat16)
        values = v_raw.astype(jnp.bfloat16)
        flat_keys = keys.reshape(rows, local_width)
        tail = (flat_keys, values, doc_ids)
        received = [
            shifted((tail[0], tail[1], tail[2]), "sp", distance_back)
            for distance_back in range(depth, 0, -1)
        ]
        ext_keys = jnp.concatenate([item[0] for item in received] + [flat_keys], axis=0)
        ext_values = jnp.concatenate([item[1] for item in received] + [values], axis=0)
        ext_docs = jnp.concatenate([item[2] for item in received] + [doc_ids], axis=0)
        ext_keys = ext_keys.reshape(reach + rows, heads_here, head_size)
        ext_values = ext_values.reshape(reach + rows, heads_here, head_size)
        attended = attend(query, ext_keys, ext_values, ext_docs, doc_ids, offset, table)
        all_heads = lax.all_gather(attended, "tp", axis=1, tiled=True)
        projected = jnp.dot(
            all_heads,
            lax.all_gather(out_weight[layer], "sp", axis=0, tiled=True),
            preferred_element_type=jnp.float32,
        )
        own_cols = lax.dynamic_slice_in_dim(widened, col_start, col_width, 1)
        new_cols = (own_cols + projected).astype(jnp.bfloat16)
        x = lax.all_gather(new_cols, "tp", axis=1, tiled=True)
    return x


def solution(mesh):
    placed = (
        P(("grp", "sp"), None),
        P(("grp", "sp")),
        P(),
        P(None, "sp", "tp"),
        P(None, "sp", "tp"),
        P(None, "sp", "tp"),
        P(None, "sp", "tp"),
        P(),
        P(),
        P("tp", None),
    )
    return jax.shard_map(
        on_device, mesh=mesh, in_specs=placed, out_specs=P(("grp", "sp"), None), check_vma=False
    )
```

profile of v0, /device:TPU:0, one launch (start us, length us, event | category | flops | bytes accessed | tf_op | source)
XLA Modules:
  0.0 338.0 jit_solution(15381538330978030332)
XLA Ops:
  6.5 2.0 fusion.257
  8.6 2.0 fusion.256
  11.6 6.0 %collective-permute-start.1 = (s32[256]{0:T(256)S(1)}, s32[256]{0:T(256)S(1)}, u32[]{:S(2)}, u32[]{:S(2)}) collective-permute-start(s32[256]{0:T(256)S(1)} %copy-done.17), channel_id=1, source_target_pairs={{0,8},{4,12},{1,9},{5,13},{2,10},{6,14},{3,11},{7,15},{16,24},{20,... | collective-permute-start | bytes 3080 | tf_op jit(solution)/shard_map/ppermute | solution.py:16
  17.5 3.5 %collective-permute-start.2 = (s32[256]{0:T(256)S(1)}, s32[256]{0:T(256)S(1)}, u32[]{:S(2)}, u32[]{:S(2)}) collective-permute-start(s32[256]{0:T(256)S(1)} %copy-done.17), channel_id=1, source_target_pairs={{0,4},{4,8},{8,12},{1,5},{5,9},{9,13},{2,6},{6,10},{10,14},{3,7},{... | collective-permute-start | bytes 3080 | tf_op jit(solution)/shard_map/ppermute | solution.py:16
  30.6 9.0 %all-gather.27.cloned.1.call-done = bf16[1,2048,256]{2,1,0:T(8,128)(2,1)} async-done(((bf16[1,512,256]{2,1,0:T(8,128)(2,1)}), bf16[1,2048,256]{2,1,0:T(8,128)(2,1)}) %all-gather.27.cloned.1.call-update) | async-done | bytes 1048592 | tf_op jit(solution)/shard_map/all_gather | solution.py:118
  39.7 1.9 bitcast_reduce_fusion.2
  41.7 3.7 %collective-permute-start.3 = (bf16[256,256]{0,1:T(8,128)(2,1)S(1)}, bf16[256,256]{0,1:T(8,128)(2,1)S(1)}, u32[]{:S(2)}, u32[]{:S(2)}) collective-permute-start(bf16[256,256]{0,1:T(8,128)(2,1)S(1)} %fusion.61), channel_id=1, source_target_pairs={{0,8},{4,12},{1,9},{5,13},{2,10},{6,14},{3,11},{7,15},{16,24},{20,... | collective-permute-start | bytes 393224 | tf_op jit(solution)/shard_map/ppermute | solution.py:16
  45.4 2.5 collective-permute-start.4
  48.0 20.7 %all-gather.23.cloned.1.call-done = bf16[1,2048,256]{2,1,0:T(8,128)(2,1)} async-done(((bf16[1,512,256]{2,1,0:T(8,128)(2,1)}), bf16[1,2048,256]{2,1,0:T(8,128)(2,1)}) %all-gather.23.cloned.1.call-update) | async-done | bytes 1048592 | tf_op jit(solution)/shard_map/all_gather | solution.py:123
  70.5 5.6 %collective-permute-start.5 = (bf16[256,256]{1,0:T(8,128)(2,1)S(1)}, bf16[256,256]{1,0:T(8,128)(2,1)S(1)}, u32[]{:S(2)}, u32[]{:S(2)}) collective-permute-start(bf16[256,256]{1,0:T(8,128)(2,1)S(1)} %convolution_convert_fusion.1), channel_id=1, source_target_pairs={{0,4},{4,8},{8,12},{1,5},{5,9},{9,13},{2,6},{6,10},{10,14},{3,7},{... | collective-permute-start | bytes 393224 | tf_op jit(solution)/shard_map/ppermute | solution.py:16
  76.1 4.3 %collective-permute-start = (bf16[256,256]{1,0:T(8,128)(2,1)S(1)}, bf16[256,256]{1,0:T(8,128)(2,1)S(1)}, u32[]{:S(2)}, u32[]{:S(2)}) collective-permute-start(bf16[256,256]{1,0:T(8,128)(2,1)S(1)} %convolution_convert_fusion.1), channel_id=1, source_target_pairs={{0,8},{4,12},{1,9},{5,13},{2,10},{6,14},{3,11},{7,15},{16,24},{20,... | collective-permute-start | bytes 393224 | tf_op jit(solution)/shard_map/ppermute | solution.py:16
  81.3 19.7 %all-gather.25.cloned.1.call-done = bf16[1,2048,256]{2,1,0:T(8,128)(2,1)} async-done(((bf16[1,512,256]{2,1,0:T(8,128)(2,1)}), bf16[1,2048,256]{2,1,0:T(8,128)(2,1)}) %all-gather.25.cloned.1.call-update) | async-done | bytes 1048592 | tf_op jit(solution)/shard_map/all_gather | solution.py:113
  101.0 1.9 bitcast_reduce_fusion.3
  118.7 3.6 %concatenate.92 = f32[4,4,64,576]{3,2,1,0:T(8,128)S(1)} concatenate(f32[4,4,64,64]{3,2,1,0:T(8,128)} %fusion.114, f32[4,4,64,64]{3,2,1,0:T(8,128)} %fusion.112, f32[4,4,64,64]{3,2,1,0:T(8,128)} %fusion.110, f32[4,4,64,64]{3,2,1,0:T(8,128)} %fusion.108, f32[4,4,64,64]{3,2,1,0:T(8,128)} %fusion.106, f32[4,4,64,64]{3,2,1,0:T(8,128)} %fusion.104, f32[4,4,64,64]{3,2,1,0:T(8,128)} %fusion.102, ...), dimensions={3} | concatenate | bytes 4718592 | tf_op jit(solution)/shard_map/concatenate | solution.py:54
  139.4 8.7 %all_gather.39 = bf16[256,1024]{1,0:T(8,128)(2,1)S(1)} all-gather(bf16[256,256]{1,0:T(8,128)(2,1)S(1)} %reshape.224), channel_id=1, replica_groups=mesh['grp'=2,'sp'=4,'tp'=4] {'tp'}, dimensions={1}, use_global_device_ids=true | all-gather | bytes 655360 | tf_op jit(solution)/shard_map/all_gather | solution.py:145
  148.1 2.5 fusion.16
  153.6 15.3 %all-gather.19.cloned.1.call-done = bf16[256,2048]{1,0:T(8,128)(2,1)} async-done(((bf16[256,512]{1,0:T(8,128)(2,1)}), bf16[256,2048]{1,0:T(8,128)(2,1)}) %all-gather.19.cloned.1.call-update) | async-done | bytes 1048592 | tf_op jit(solution)/shard_map/all_gather | solution.py:153
  170.4 27.9 %all-gather.35.cloned.1.call-done = bf16[1,2048,256]{2,1,0:T(8,128)(2,1)} async-done(((bf16[1,512,256]{2,1,0:T(8,128)(2,1)}), bf16[1,2048,256]{2,1,0:T(8,128)(2,1)}) %all-gather.35.cloned.1.call-update) | async-done | bytes 1048592 | tf_op jit(solution)/shard_map/all_gather | solution.py:118
  198.3 2.2 bitcast_reduce_fusion
  200.6 3.7 %collective-permute-start.7 = (bf16[256,256]{0,1:T(8,128)(2,1)S(1)}, bf16[256,256]{0,1:T(8,128)(2,1)S(1)}, u32[]{:S(2)}, u32[]{:S(2)}) collective-permute-start(bf16[256,256]{0,1:T(8,128)(2,1)S(1)} %fusion.59), channel_id=1, source_target_pairs={{0,8},{4,12},{1,9},{5,13},{2,10},{6,14},{3,11},{7,15},{16,24},{20,... | collective-permute-start | bytes 393224 | tf_op jit(solution)/shard_map/ppermute | solution.py:16
  204.4 3.1 collective-permute-start.8
  207.7 19.0 %all-gather.31.cloned.1.call-done = bf16[1,2048,256]{2,1,0:T(8,128)(2,1)} async-done(((bf16[1,512,256]{2,1,0:T(8,128)(2,1)}), bf16[1,2048,256]{2,1,0:T(8,128)(2,1)}) %all-gather.31.cloned.1.call-update) | async-done | bytes 1048592 | tf_op jit(solution)/shard_map/all_gather | solution.py:123
  226.7 2.4 convolution_convert_fusion
  229.1 7.3 %collective-permute-start.9 = (bf16[256,256]{1,0:T(8,128)(2,1)}, bf16[256,256]{1,0:T(8,128)(2,1)}, u32[]{:S(2)}, u32[]{:S(2)}) collective-permute-start(bf16[256,256]{1,0:T(8,128)(2,1)} %convolution_convert_fusion), channel_id=1, source_target_pairs={{0,4},{4,8},{8,12},{1,5},{5,9},{9,13},{2,6},{6,10},{10,14},{3,7},{... | collective-permute-start | bytes 393224 | tf_op jit(solution)/shard_map/ppermute | solution.py:16
  236.4 4.2 %collective-permute-start.6 = (bf16[256,256]{1,0:T(8,128)(2,1)}, bf16[256,256]{1,0:T(8,128)(2,1)}, u32[]{:S(2)}, u32[]{:S(2)}) collective-permute-start(bf16[256,256]{1,0:T(8,128)(2,1)} %convolution_convert_fusion), channel_id=1, source_target_pairs={{0,8},{4,12},{1,9},{5,13},{2,10},{6,14},{3,11},{7,15},{16,24},{20,... | collective-permute-start | bytes 393224 | tf_op jit(solution)/shard_map/ppermute | solution.py:16
  242.4 18.9 %all-gather.33.cloned.1.call-done = bf16[1,2048,256]{2,1,0:T(8,128)(2,1)} async-done(((bf16[1,512,256]{2,1,0:T(8,128)(2,1)}), bf16[1,2048,256]{2,1,0:T(8,128)(2,1)}) %all-gather.33.cloned.1.call-update) | async-done | bytes 1048592 | tf_op jit(solution)/shard_map/all_gather | solution.py:113
  278.4 3.6 %concatenate.98 = f32[4,4,64,576]{3,2,1,0:T(8,128)S(1)} concatenate(f32[4,4,64,64]{3,2,1,0:T(8,128)} %fusion.87, f32[4,4,64,64]{3,2,1,0:T(8,128)} %fusion.85, f32[4,4,64,64]{3,2,1,0:T(8,128)} %fusion.83, f32[4,4,64,64]{3,2,1,0:T(8,128)} %fusion.81, f32[4,4,64,64]{3,2,1,0:T(8,128)} %fusion.79, f32[4,4,64,64]{3,2,1,0:T(8,128)} %fusion.77, f32[4,4,64,64]{3,2,1,0:T(8,128)} %fusion.75, ...), dimensions={3} | concatenate | bytes 4718592 | tf_op jit(solution)/shard_map/concatenate | solution.py:54
  282.0 2.3 fusion.267
  299.8 8.3 %all_gather.45 = bf16[256,1024]{1,0:T(8,128)(2,1)S(1)} all-gather(bf16[256,256]{1,0:T(8,128)(2,1)S(1)} %reshape.226), channel_id=1, replica_groups=mesh['grp'=2,'sp'=4,'tp'=4] {'tp'}, dimensions={1}, use_global_device_ids=true | all-gather | bytes 655360 | tf_op jit(solution)/shard_map/all_gather | solution.py:145
  308.1 2.5 fusion.17
  310.7 18.2 %all-gather.21.cloned.1.call-done = bf16[256,2048]{1,0:T(8,128)(2,1)} async-done(((bf16[256,512]{1,0:T(8,128)(2,1)}), bf16[256,2048]{1,0:T(8,128)(2,1)}) %all-gather.21.cloned.1.call-update) | async-done | bytes 1048592 | tf_op jit(solution)/shard_map/all_gather | solution.py:153
  328.9 2.3 copy.233
  (275 shorter events, 84.8 us)
Async XLA Ops:
  6.5 4.1 %copy-start.12 = (bf16[2,512,256]{2,1,0:T(8,128)(2,1)S(1)}, bf16[2,512,256]{2,1,0:T(8,128)(2,1)}, u32[]{:S(2)}) copy-start(bf16[2,512,256]{2,1,0:T(8,128)(2,1)} %param.13) | copy-start | bytes 1572868
  6.5 5.0 %copy-start.17 = (s32[256]{0:T(256)S(1)}, s32[256]{0:T(256)}, u32[]{:S(2)}) copy-start(s32[256]{0:T(256)} %param.11) | copy-start | bytes 3076
  6.5 14.5 %copy-start.13 = (bf16[2,256,512]{2,1,0:T(8,128)(2,1)S(1)}, bf16[2,256,512]{2,1,0:T(8,128)(2,1)}, u32[]{:S(2)}) copy-start(bf16[2,256,512]{2,1,0:T(8,128)(2,1)} %param.16) | copy-start | bytes 1572868
  6.5 33.1 %all-gather.27.cloned.1.call-start = ((), (), s32[]{:S(2)}) async-start(), calls=%async_computation.4 | async-start | bytes 1310720 | tf_op jit(solution)/shard_map/all_gather | solution.py:118
  8.5 13.5 %copy-start.16 = (f32[4,513]{1,0:T(4,128)S(1)}, f32[4,513]{1,0:T(4,128)}, u32[]{:S(2)}) copy-start(f32[4,513]{1,0:T(4,128)} %param.19) | copy-start | bytes 24628
  8.5 13.7 %copy-start.15 = (f32[2,2048]{1,0:T(2,128)S(1)}, f32[2,2048]{1,0:T(2,128)}, u32[]{:S(2)}) copy-start(f32[2,2048]{1,0:T(2,128)} %param.12) | copy-start | bytes 49156
  8.5 13.7 %copy-start.3 = (bf16[256,2048]{1,0:T(8,128)(2,1)S(1)}, bf16[256,2048]{1,0:T(8,128)(2,1)}, u32[]{:S(2)}) copy-start(bf16[256,2048]{1,0:T(8,128)(2,1)} %param.10) | copy-start | bytes 3145732
  8.5 60.2 %all-gather.23.cloned.1.call-start = ((), (), s32[]{:S(2)}) async-start(), calls=%async_computation.2 | async-start | bytes 1310720 | tf_op jit(solution)/shard_map/all_gather | solution.py:123
  10.5 12.0 %copy-start.18 = (f32[2,64]{1,0:T(2,128)S(1)}, f32[2,64]{1,0:T(2,128)}, u32[]{:S(2)}) copy-start(f32[2,64]{1,0:T(2,128)} %param.17) | copy-start | bytes 1540
  10.5 12.0 %copy-start.19 = (f32[2,64]{1,0:T(2,128)S(1)}, f32[2,64]{1,0:T(2,128)}, u32[]{:S(2)}) copy-start(f32[2,64]{1,0:T(2,128)} %param.18) | copy-start | bytes 1540
  10.6 90.5 %all-gather.25.cloned.1.call-start = ((), (), s32[]{:S(2)}) async-start(), calls=%async_computation.3 | async-start | bytes 1310720 | tf_op jit(solution)/shard_map/all_gather | solution.py:113
  11.5 136.6 %all-gather.29.cloned.1.call-start = ((), (), s32[]{:S(2)}) async-start(), calls=%async_computation.5 | async-start | bytes 1310720 | tf_op jit(solution)/shard_map/all_gather | solution.py:148
  11.6 18.6 %collective-permute-start.1 = (s32[256]{0:T(256)S(1)}, s32[256]{0:T(256)S(1)}, u32[]{:S(2)}, u32[]{:S(2)}) collective-permute-start(s32[256]{0:T(256)S(1)} %copy-done.17), channel_id=1, source_target_pairs={{0,8},{4,12},{1,9},{5,13},{2,10},{6,14},{3,11},{7,15},{16,24},{20,... | collective-permute-start | bytes 3080 | tf_op jit(solution)/shard_map/ppermute | solution.py:16
  17.5 12.7 %collective-permute-start.2 = (s32[256]{0:T(256)S(1)}, s32[256]{0:T(256)S(1)}, u32[]{:S(2)}, u32[]{:S(2)}) collective-permute-start(s32[256]{0:T(256)S(1)} %copy-done.17), channel_id=1, source_target_pairs={{0,4},{4,8},{8,12},{1,5},{5,9},{9,13},{2,6},{6,10},{10,14},{3,7},{... | collective-permute-start | bytes 3080 | tf_op jit(solution)/shard_map/ppermute | solution.py:16
  21.9 147.0 %all-gather.19.cloned.1.call-start = ((), (), s32[]{:S(2)}) async-start(), calls=%async_computation | async-start | bytes 1310720 | tf_op jit(solution)/shard_map/all_gather | solution.py:153
  30.6 91.7 %copy-start.5 = (pred[4,64,576]{2,1,0:T(8,128)(4,1)}, pred[4,64,576]{2,1,0:T(8,128)(4,1)S(1)}, u32[]{:S(2)}) copy-start(pred[4,64,576]{2,1,0:T(8,128)(4,1)S(1)} %compare_and_fusion) | copy-start | bytes 442372
  41.7 63.0 %collective-permute-start.3 = (bf16[256,256]{0,1:T(8,128)(2,1)S(1)}, bf16[256,256]{0,1:T(8,128)(2,1)S(1)}, u32[]{:S(2)}, u32[]{:S(2)}) collective-permute-start(bf16[256,256]{0,1:T(8,128)(2,1)S(1)} %fusion.61), channel_id=1, source_target_pairs={{0,8},{4,12},{1,9},{5,13},{2,10},{6,14},{3,11},{7,15},{16,24},{20,... | collective-permute-start | bytes 393224 | tf_op jit(solution)/shard_map/ppermute | solution.py:16
  45.4 60.5 %collective-permute-start.4 = (bf16[256,256]{0,1:T(8,128)(2,1)S(1)}, bf16[256,256]{0,1:T(8,128)(2,1)S(1)}, u32[]{:S(2)}, u32[]{:S(2)}) collective-permute-start(bf16[256,256]{0,1:T(8,128)(2,1)S(1)} %fusion.61), channel_id=1, source_target_pairs={{0,4},{4,8},{8,12},{1,5},{5,9},{9,13},{2,6},{6,10},{10,14},{3,7},{... | collective-permute-start | bytes 393224 | tf_op jit(solution)/shard_map/ppermute | solution.py:16
  70.5 44.1 %collective-permute-start.5 = (bf16[256,256]{1,0:T(8,128)(2,1)S(1)}, bf16[256,256]{1,0:T(8,128)(2,1)S(1)}, u32[]{:S(2)}, u32[]{:S(2)}) collective-permute-start(bf16[256,256]{1,0:T(8,128)(2,1)S(1)} %convolution_convert_fusion.1), channel_id=1, source_target_pairs={{0,4},{4,8},{8,12},{1,5},{5,9},{9,13},{2,6},{6,10},{10,14},{3,7},{... | collective-permute-start | bytes 393224 | tf_op jit(solution)/shard_map/ppermute | solution.py:16
  76.1 38.5 %collective-permute-start = (bf16[256,256]{1,0:T(8,128)(2,1)S(1)}, bf16[256,256]{1,0:T(8,128)(2,1)S(1)}, u32[]{:S(2)}, u32[]{:S(2)}) collective-permute-start(bf16[256,256]{1,0:T(8,128)(2,1)S(1)} %convolution_convert_fusion.1), channel_id=1, source_target_pairs={{0,8},{4,12},{1,9},{5,13},{2,10},{6,14},{3,11},{7,15},{16,24},{20,... | collective-permute-start | bytes 393224 | tf_op jit(solution)/shard_map/ppermute | solution.py:16
  150.6 47.7 %all-gather.35.cloned.1.call-start = ((), (), s32[]{:S(2)}) async-start(), calls=%async_computation.8 | async-start | bytes 1310720 | tf_op jit(solution)/shard_map/all_gather | solution.py:118
  151.2 75.5 %all-gather.31.cloned.1.call-start = ((), (), s32[]{:S(2)}) async-start(), calls=%async_computation.6 | async-start | bytes 1310720 | tf_op jit(solution)/shard_map/all_gather | solution.py:123
  152.0 109.3 %all-gather.33.cloned.1.call-start = ((), (), s32[]{:S(2)}) async-start(), calls=%async_computation.7 | async-start | bytes 1310720 | tf_op jit(solution)/shard_map/all_gather | solution.py:113
  152.7 155.4 %all-gather.37.cloned.1.call-start = ((), (), s32[]{:S(2)}) async-start(), calls=%async_computation.9 | async-start | bytes 1310720 | tf_op jit(solution)/shard_map/all_gather | solution.py:148
  153.4 175.5 %all-gather.21.cloned.1.call-start = ((), (), s32[]{:S(2)}) async-start(), calls=%async_computation.1 | async-start | bytes 1310720 | tf_op jit(solution)/shard_map/all_gather | solution.py:153
  170.4 56.3 %copy-start.4 = (bf16[256,2048]{1,0:T(8,128)(2,1)S(1)}, bf16[256,2048]{1,0:T(8,128)(2,1)}, u32[]{:S(2)}) copy-start(bf16[256,2048]{1,0:T(8,128)(2,1)} %all-gather.19.cloned.1.call-done) | copy-start | bytes 3145732
  200.6 65.9 %collective-permute-start.7 = (bf16[256,256]{0,1:T(8,128)(2,1)S(1)}, bf16[256,256]{0,1:T(8,128)(2,1)S(1)}, u32[]{:S(2)}, u32[]{:S(2)}) collective-permute-start(bf16[256,256]{0,1:T(8,128)(2,1)S(1)} %fusion.59), channel_id=1, source_target_pairs={{0,8},{4,12},{1,9},{5,13},{2,10},{6,14},{3,11},{7,15},{16,24},{20,... | collective-permute-start | bytes 393224 | tf_op jit(solution)/shard_map/ppermute | solution.py:16
  204.4 63.4 %collective-permute-start.8 = (bf16[256,256]{0,1:T(8,128)(2,1)S(1)}, bf16[256,256]{0,1:T(8,128)(2,1)}, u32[]{:S(2)}, u32[]{:S(2)}) collective-permute-start(bf16[256,256]{0,1:T(8,128)(2,1)S(1)} %fusion.59), channel_id=1, source_target_pairs={{0,4},{4,8},{8,12},{1,5},{5,9},{9,13},{2,6},{6,10},{10,14},{3,7},{... | collective-permute-start | bytes 393224 | tf_op jit(solution)/shard_map/ppermute | solution.py:16
  229.1 56.4 %collective-permute-start.9 = (bf16[256,256]{1,0:T(8,128)(2,1)}, bf16[256,256]{1,0:T(8,128)(2,1)}, u32[]{:S(2)}, u32[]{:S(2)}) collective-permute-start(bf16[256,256]{1,0:T(8,128)(2,1)} %convolution_convert_fusion), channel_id=1, source_target_pairs={{0,4},{4,8},{8,12},{1,5},{5,9},{9,13},{2,6},{6,10},{10,14},{3,7},{... | collective-permute-start | bytes 393224 | tf_op jit(solution)/shard_map/ppermute | solution.py:16
  236.4 48.0 %collective-permute-start.6 = (bf16[256,256]{1,0:T(8,128)(2,1)}, bf16[256,256]{1,0:T(8,128)(2,1)}, u32[]{:S(2)}, u32[]{:S(2)}) collective-permute-start(bf16[256,256]{1,0:T(8,128)(2,1)} %convolution_convert_fusion), channel_id=1, source_target_pairs={{0,8},{4,12},{1,9},{5,13},{2,10},{6,14},{3,11},{7,15},{16,24},{20,... | collective-permute-start | bytes 393224 | tf_op jit(solution)/shard_map/ppermute | solution.py:16
  278.4 3.6 %copy-start.6 = (pred[4,64,576]{2,1,0:T(8,128)(4,1)S(1)}, pred[4,64,576]{2,1,0:T(8,128)(4,1)}, u32[]{:S(2)}) copy-start(pred[4,64,576]{2,1,0:T(8,128)(4,1)} %copy-done.5) | copy-start | bytes 442372
  284.4 5.1 %copy-start = (f32[4,4,64,576]{3,2,1,0:T(8,128)S(1)}, f32[4,4,64,576]{3,2,1,0:T(8,128)}, u32[]{:S(2)}) copy-start(f32[4,4,64,576]{3,2,1,0:T(8,128)} %get-tuple-element.66) | copy-start | bytes 7077892
  (8 other events, 14.1 us)
Sparse Core Ops, SparseCore 0:
  8.9 30.7 all-gather.26
  41.2 27.4 all-gather.22
  70.3 30.6 all-gather.24
  102.4 31.1 all-gather.28
  150.8 18.0 all-gather.18
  170.3 27.9 all-gather.34
  199.9 26.7 all-gather.30
  228.2 32.9 all-gather.32
  262.8 30.7 all-gather.36
  310.8 18.0 all-gather.20
where the time goes:
time: 339 us; the launch traced here: 338 us
  waiting for transfers between devices  152 us (45%)
  matrix products  46.2 us (14%)
  local copies, waits for them, and re-layouts  45.6 us (13%)
  starting transfers between devices  44.3 us (13%)
  other arithmetic  19 us (6%)
  blocking collectives  17.1 us (5%)
  between operations  14.4 us (4%)
    ppermute x10, starting transfers between devices, shifted(): lax.ppermute(value, axis, [(source, source + steps) for source in range(i...  43.9 us
    all_gather x2, waiting for transfers between devices, on_device(): lax.all_gather(value_weight[layer], 'sp', axis=0, tiled=True)  39.8 us
    all_gather x2, waiting for transfers between devices, on_device(): lax.all_gather(query_weight[layer], 'sp', axis=0, tiled=True)  38.6 us
    all_gather x2, waiting for transfers between devices, on_device(): lax.all_gather(key_weight[layer], 'sp', axis=0, tiled=True)  37 us
    all_gather x2, waiting for transfers between devices, on_device(): x = lax.all_gather(new_cols, 'tp', axis=1, tiled=True)  33.5 us
    slice x20, local copies, waits for them, and re-layouts, attend(): value_blocks[earlier:earlier + count]  20.2 us
    dot_general x18, matrix products, attend(): jnp.einsum('nqhd,nkhd->nhqk', blocks, key_blocks[earlier:earlier + count]...  18.4 us
    all_gather x2, blocking collectives, on_device(): all_heads = lax.all_gather(attended, 'tp', axis=1, tiled=True)  17.1 us
  transfers between devices with their start and end apart: 20, of which 8 were waited for; matrix products, arithmetic and copies ran while one was open for 29% of the time, Pallas kernels for 0%

commit v1 on v0

--- a/solution.py
+++ b/solution.py
@@ -1,13 +1,32 @@
+import functools
 import jax
 import jax.numpy as jnp
 from jax import lax
 from jax.sharding import PartitionSpec as P
+from jax.lax import axis_index, axis_size, ppermute
 
 SEG = 64
 LEFT = 8
 MAXREL = 256
 LAYERS = 2
 epsilon = 1e-06
+
+
+def _get_run(w_in, mesh_name, axis_no):
+    fan = axis_size(mesh_name)
+    inbox = tuple(((j0, (j0 + 1) % fan) for j0 in range(fan)))
+    carry_out = [None] * fan
+    carry_out[fan - 1] = w_in
+    for i0 in range(fan - 2, -1, -1):
+        carry_out[i0] = ppermute(carry_out[i0 + 1], mesh_name, inbox)
+    return jnp.roll(
+        jnp.concatenate(carry_out, axis=axis_no),
+        shift=(axis_index(mesh_name) + 1) * w_in.shape[axis_no],
+        axis=axis_no,
+    )
+
+
+get_sites = functools.partial(_get_run, mesh_name="tp", axis_no=1)
 
 
 def shifted(value, axis, steps):
@@ -150,7 +169,7 @@
         )
         own_cols = lax.dynamic_slice_in_dim(widened, col_start, col_width, 1)
         new_cols = (own_cols + projected).astype(jnp.bfloat16)
-        x = lax.all_gather(new_cols, "tp", axis=1, tiled=True)
+        x = get_sites(new_cols)
     return x
 
 

time: 339 us -> 322 us (0.950)
  waiting for transfers between devices: 152 us -> 119 us
  other arithmetic: 19 us -> 25.6 us
  local copies, waits for them, and re-layouts: 45.6 us -> 49.8 us
  starting transfers between devices: 44.3 us -> 48.1 us
    ppermute x0 -> x6, waiting for transfers between devices: none -> 33.9 us  [_get_run(): carry_out[i0] = ppermute(carry_out[i0 + 1], mesh_name, inbox)]
    all_gather x2 -> x0, waiting for transfers between devices: 33.5 us -> none  [on_device(): x = lax.all_gather(new_cols, 'tp', axis=1, tiled=True)]
    all_gather x2, waiting for transfers between devices: 37 us -> 7.7 us  [on_device(): lax.all_gather(key_weight[layer], 'sp', axis=0, tiled=True)]
    slice x20, local copies, waits for them, and re-layouts: 4 us -> 8.17 us  [attend(): key_blocks[earlier:earlier + count]]
    dot_general x18, matrix products: 10.9 us -> 14.7 us  [attend(): jnp.einsum('nhqk,nkhd->nqhd', part_weights, value_blocks[earlier:earlier...]
  transfers between devices with their start and end apart: 20 -> 24, of which waited for: 8 -> 11; matrix products, arithmetic and copies ran while one was open for 29% -> 37% of each run, Pallas kernels for 0% -> 0%
where the time goes in v1:
time: 322 us; the launch traced here: 321 us
  waiting for transfers between devices  119 us (37%)
  local copies, waits for them, and re-layouts  49.8 us (15%)
  matrix products  48.9 us (15%)
  starting transfers between devices  48.1 us (15%)
  other arithmetic  25.6 us (8%)
  blocking collectives  15.4 us (5%)
  between operations  14.4 us (4%)
    ppermute x10, starting transfers between devices, shifted(): lax.ppermute(value, axis, [(source, source + steps) for source in range(i...  47 us
    all_gather x2, waiting for transfers between devices, on_device(): lax.all_gather(query_weight[layer], 'sp', axis=0, tiled=True)  38.6 us
    all_gather x2, waiting for transfers between devices, on_device(): lax.all_gather(value_weight[layer], 'sp', axis=0, tiled=True)  37.2 us
    ppermute x6, waiting for transfers between devices, _get_run(): carry_out[i0] = ppermute(carry_out[i0 + 1], mesh_name, inbox)  33.9 us
    slice x20, local copies, waits for them, and re-layouts, attend(): value_blocks[earlier:earlier + count]  19.7 us
    dot_general x18, matrix products, attend(): jnp.einsum('nqhd,nkhd->nhqk', blocks, key_blocks[earlier:earlier + count]...  18.7 us
    all_gather x2, blocking collectives, on_device(): all_heads = lax.all_gather(attended, 'tp', axis=1, tiled=True)  15.4 us
    dot_general x18, matrix products, attend(): jnp.einsum('nhqk,nkhd->nqhd', part_weights, value_blocks[earlier:earlier...  14.7 us
  transfers between devices with their start and end apart: 24, of which 11 were waited for; matrix products, arithmetic and copies ran while one was open for 37% of the time, Pallas kernels for 0%

profile of v1, /device:TPU:0, one launch (start us, length us, event | category | flops | bytes accessed | tf_op | source)
XLA Modules:
  0.0 320.9 jit_solution(4386245361868567081)
XLA Ops:
  13.6 6.0 %collective-permute-start.1 = (s32[256]{0:T(256)S(1)}, s32[256]{0:T(256)S(1)}, u32[]{:S(2)}, u32[]{:S(2)}) collective-permute-start(s32[256]{0:T(256)S(1)} %copy-done.27), channel_id=1, source_target_pairs={{0,8},{4,12},{1,9},{5,13},{2,10},{6,14},{3,11},{7,15},{16,24},{20,... | collective-permute-start | bytes 3080 | tf_op jit(solution)/shard_map/ppermute | solution.py:35
  19.6 3.5 %collective-permute-start.2 = (s32[256]{0:T(256)S(1)}, s32[256]{0:T(256)S(1)}, u32[]{:S(2)}, u32[]{:S(2)}) collective-permute-start(s32[256]{0:T(256)S(1)} %copy-done.27), channel_id=1, source_target_pairs={{0,4},{4,8},{8,12},{1,5},{5,9},{9,13},{2,6},{6,10},{10,14},{3,7},{... | collective-permute-start | bytes 3080 | tf_op jit(solution)/shard_map/ppermute | solution.py:35
  31.9 7.7 %all-gather.21.cloned.1.call-done = bf16[1,2048,256]{2,1,0:T(8,128)(2,1)} async-done(((bf16[1,512,256]{2,1,0:T(8,128)(2,1)}), bf16[1,2048,256]{2,1,0:T(8,128)(2,1)}) %all-gather.21.cloned.1.call-update) | async-done | bytes 1048592 | tf_op jit(solution)/shard_map/all_gather | solution.py:137
  41.6 3.8 %collective-permute-start.3 = (bf16[256,256]{0,1:T(8,128)(2,1)S(1)}, bf16[256,256]{0,1:T(8,128)(2,1)S(1)}, u32[]{:S(2)}, u32[]{:S(2)}) collective-permute-start(bf16[256,256]{0,1:T(8,128)(2,1)S(1)} %fusion.76), channel_id=1, source_target_pairs={{0,8},{4,12},{1,9},{5,13},{2,10},{6,14},{3,11},{7,15},{16,24},{20,... | collective-permute-start | bytes 393224 | tf_op jit(solution)/shard_map/ppermute | solution.py:35
  45.4 2.4 collective-permute-start.4
  48.1 20.3 %all-gather.17.cloned.1.call-done = bf16[1,2048,256]{2,1,0:T(8,128)(2,1)} async-done(((bf16[1,512,256]{2,1,0:T(8,128)(2,1)}), bf16[1,2048,256]{2,1,0:T(8,128)(2,1)}) %all-gather.17.cloned.1.call-update) | async-done | bytes 1048592 | tf_op jit(solution)/shard_map/all_gather | solution.py:142
  70.1 6.1 %collective-permute-start.5 = (bf16[256,256]{1,0:T(8,128)(2,1)S(1)}, bf16[256,256]{1,0:T(8,128)(2,1)S(1)}, u32[]{:S(2)}, u32[]{:S(2)}) collective-permute-start(bf16[256,256]{1,0:T(8,128)(2,1)S(1)} %convolution_convert_fusion.1), channel_id=1, source_target_pairs={{0,4},{4,8},{8,12},{1,5},{5,9},{9,13},{2,6},{6,10},{10,14},{3,7},{... | collective-permute-start | bytes 393224 | tf_op jit(solution)/shard_map/ppermute | solution.py:35
  76.2 4.3 %collective-permute-start = (bf16[256,256]{1,0:T(8,128)(2,1)S(1)}, bf16[256,256]{1,0:T(8,128)(2,1)S(1)}, u32[]{:S(2)}, u32[]{:S(2)}) collective-permute-start(bf16[256,256]{1,0:T(8,128)(2,1)S(1)} %convolution_convert_fusion.1), channel_id=1, source_target_pairs={{0,8},{4,12},{1,9},{5,13},{2,10},{6,14},{3,11},{7,15},{16,24},{20,... | collective-permute-start | bytes 393224 | tf_op jit(solution)/shard_map/ppermute | solution.py:35
  81.4 19.7 %all-gather.19.cloned.1.call-done = bf16[1,2048,256]{2,1,0:T(8,128)(2,1)} async-done(((bf16[1,512,256]{2,1,0:T(8,128)(2,1)}), bf16[1,2048,256]{2,1,0:T(8,128)(2,1)}) %all-gather.19.cloned.1.call-update) | async-done | bytes 1048592 | tf_op jit(solution)/shard_map/all_gather | solution.py:132
  118.0 3.6 %concatenate.101 = f32[4,4,64,576]{3,2,1,0:T(8,128)S(1)} concatenate(f32[4,4,64,64]{3,2,1,0:T(8,128)} %fusion.129, f32[4,4,64,64]{3,2,1,0:T(8,128)} %fusion.127, f32[4,4,64,64]{3,2,1,0:T(8,128)} %fusion.125, f32[4,4,64,64]{3,2,1,0:T(8,128)} %fusion.123, f32[4,4,64,64]{3,2,1,0:T(8,128)} %fusion.121, f32[4,4,64,64]{3,2,1,0:T(8,128)} %fusion.119, f32[4,4,64,64]{3,2,1,0:T(8,128)} %fusion.117, ...), dimensions={3} | concatenate | bytes 4718592 | tf_op jit(solution)/shard_map/concatenate | solution.py:73
  131.7 8.7 %all_gather.33 = bf16[256,1024]{1,0:T(8,128)(2,1)S(1)} all-gather(bf16[256,256]{1,0:T(8,128)(2,1)S(1)} %reshape.224), channel_id=1, replica_groups=mesh['grp'=2,'sp'=4,'tp'=4] {'tp'}, dimensions={1}, use_global_device_ids=true | all-gather | bytes 655360 | tf_op jit(solution)/shard_map/all_gather | solution.py:164
  142.7 5.4 %collective-permute-done.6 = bf16[256,512]{1,0:T(8,128)(2,1)S(1)} collective-permute-done((bf16[256,512]{1,0:T(8,128)(2,1)S(1)}, bf16[256,512]{1,0:T(8,128)(2,1)S(1)}, u32[]{:S(2)}, u32[]{:S(2)}) %collective-permute-start.6) | collective-permute-done | bytes 262176 | tf_op jit(solution)/shard_map/ppermute | solution.py:21
  148.1 5.8 %collective-permute-done.7 = bf16[256,512]{1,0:T(8,128)(2,1)S(1)} collective-permute-done((bf16[256,512]{1,0:T(8,128)(2,1)S(1)}, bf16[256,512]{1,0:T(8,128)(2,1)S(1)}, u32[]{:S(2)}, u32[]{:S(2)}) %collective-permute-start.7) | collective-permute-done | bytes 262176 | tf_op jit(solution)/shard_map/ppermute | solution.py:21
  154.1 5.7 %collective-permute-done.8 = bf16[256,512]{1,0:T(8,128)(2,1)S(1)} collective-permute-done((bf16[256,512]{1,0:T(8,128)(2,1)S(1)}, bf16[256,512]{1,0:T(8,128)(2,1)S(1)}, u32[]{:S(2)}, u32[]{:S(2)}) %collective-permute-start.8) | collective-permute-done | bytes 262176 | tf_op jit(solution)/shard_map/ppermute | solution.py:21
  159.7 3.0 multiply_reduce_fusion
  164.9 5.8 %collective-permute-start.10 = (bf16[256,256]{0,1:T(8,128)(2,1)S(1)}, bf16[256,256]{0,1:T(8,128)(2,1)}, u32[]{:S(2)}, u32[]{:S(2)}) collective-permute-start(bf16[256,256]{0,1:T(8,128)(2,1)S(1)} %fusion.74), channel_id=1, source_target_pairs={{0,8},{4,12},{1,9},{5,13},{2,10},{6,14},{3,11},{7,15},{16,24},{20,... | collective-permute-start | bytes 393224 | tf_op jit(solution)/shard_map/ppermute | solution.py:35
  170.7 3.9 %collective-permute-start.11 = (bf16[256,256]{0,1:T(8,128)(2,1)S(1)}, bf16[256,256]{0,1:T(8,128)(2,1)}, u32[]{:S(2)}, u32[]{:S(2)}) collective-permute-start(bf16[256,256]{0,1:T(8,128)(2,1)S(1)} %fusion.74), channel_id=1, source_target_pairs={{0,4},{4,8},{8,12},{1,5},{5,9},{9,13},{2,6},{6,10},{10,14},{3,7},{... | collective-permute-start | bytes 393224 | tf_op jit(solution)/shard_map/ppermute | solution.py:35
  175.5 16.9 %all-gather.25.cloned.1.call-done = bf16[1,2048,256]{2,1,0:T(8,128)(2,1)} async-done(((bf16[1,512,256]{2,1,0:T(8,128)(2,1)}), bf16[1,2048,256]{2,1,0:T(8,128)(2,1)}) %all-gather.25.cloned.1.call-update) | async-done | bytes 1048592 | tf_op jit(solution)/shard_map/all_gather | solution.py:142
  192.4 2.3 convolution_convert_fusion
  194.7 6.1 %collective-permute-start.12 = (bf16[256,256]{1,0:T(8,128)(2,1)}, bf16[256,256]{1,0:T(8,128)(2,1)}, u32[]{:S(2)}, u32[]{:S(2)}) collective-permute-start(bf16[256,256]{1,0:T(8,128)(2,1)} %convolution_convert_fusion), channel_id=1, source_target_pairs={{0,4},{4,8},{8,12},{1,5},{5,9},{9,13},{2,6},{6,10},{10,14},{3,7},{... | collective-permute-start | bytes 393224 | tf_op jit(solution)/shard_map/ppermute | solution.py:35
  200.8 5.1 %collective-permute-start.9 = (bf16[256,256]{1,0:T(8,128)(2,1)}, bf16[256,256]{1,0:T(8,128)(2,1)}, u32[]{:S(2)}, u32[]{:S(2)}) collective-permute-start(bf16[256,256]{1,0:T(8,128)(2,1)} %convolution_convert_fusion), channel_id=1, source_target_pairs={{0,8},{4,12},{1,9},{5,13},{2,10},{6,14},{3,11},{7,15},{16,24},{20,... | collective-permute-start | bytes 393224 | tf_op jit(solution)/shard_map/ppermute | solution.py:35
  207.7 18.9 %all-gather.27.cloned.1.call-done = bf16[1,2048,256]{2,1,0:T(8,128)(2,1)} async-done(((bf16[1,512,256]{2,1,0:T(8,128)(2,1)}), bf16[1,2048,256]{2,1,0:T(8,128)(2,1)}) %all-gather.27.cloned.1.call-update) | async-done | bytes 1048592 | tf_op jit(solution)/shard_map/all_gather | solution.py:132
  226.6 2.5 bitcast_reduce_fusion.1
  248.8 4.7 %concatenate.108 = f32[4,4,64,576]{3,2,1,0:T(8,128)} concatenate(f32[4,4,64,64]{3,2,1,0:T(8,128)} %fusion.102, f32[4,4,64,64]{3,2,1,0:T(8,128)} %fusion.100, f32[4,4,64,64]{3,2,1,0:T(8,128)} %fusion.98, f32[4,4,64,64]{3,2,1,0:T(8,128)} %fusion.96, f32[4,4,64,64]{3,2,1,0:T(8,128)} %fusion.94, f32[4,4,64,64]{3,2,1,0:T(8,128)} %fusion.92, f32[4,4,64,64]{3,2,1,0:T(8,128)} %fusion.90, ...), dimensions={3} | concatenate | bytes 4718592 | tf_op jit(solution)/shard_map/concatenate | solution.py:73
  253.6 4.1 %fusion.283 = (f32[4,4,64]{2,1,0:T(4,128)S(1)}, f32[4,4,64,576]{3,2,1,0:T(8,128)}) fusion(f32[4,4,64,576]{3,2,1,0:T(8,128)} %concatenate.108, f32[4,64,576]{2,1,0:T(8,128)S(1)} %copy-done.1, pred[4,64,576]{2,1,0:T(8,128)(4,1)S(1)} %copy-done.4), kind=kOutput, calls=%fused_computation.567 | output fusion | flops 2949695 | bytes 5459968 | tf_op jit(solution)/shard_map/sub | solution.py:89
  263.7 2.0 divide_convert_fusion
  269.8 2.5 fusion.13
  286.0 6.7 %all_gather.38 = bf16[256,1024]{1,0:T(8,128)(2,1)S(1)} all-gather(bf16[256,256]{1,0:T(8,128)(2,1)S(1)} %reshape.226), channel_id=1, replica_groups=mesh['grp'=2,'sp'=4,'tp'=4] {'tp'}, dimensions={1}, use_global_device_ids=true | all-gather | bytes 655360 | tf_op jit(solution)/shard_map/all_gather | solution.py:164
  294.8 5.4 %collective-permute-done.13 = bf16[256,512]{1,0:T(8,128)(2,1)S(1)} collective-permute-done((bf16[256,512]{1,0:T(8,128)(2,1)S(1)}, bf16[256,512]{1,0:T(8,128)(2,1)S(1)}, u32[]{:S(2)}, u32[]{:S(2)}) %collective-permute-start.13) | collective-permute-done | bytes 262176 | tf_op jit(solution)/shard_map/ppermute | solution.py:21
  300.2 5.8 %collective-permute-done.14 = bf16[256,512]{1,0:T(8,128)(2,1)S(1)} collective-permute-done((bf16[256,512]{1,0:T(8,128)(2,1)S(1)}, bf16[256,512]{1,0:T(8,128)(2,1)S(1)}, u32[]{:S(2)}, u32[]{:S(2)}) %collective-permute-start.14) | collective-permute-done | bytes 262176 | tf_op jit(solution)/shard_map/ppermute | solution.py:21
  306.0 5.8 %collective-permute-done.15 = bf16[256,512]{1,0:T(8,128)(2,1)S(1)} collective-permute-done((bf16[256,512]{1,0:T(8,128)(2,1)S(1)}, bf16[256,512]{1,0:T(8,128)(2,1)S(1)}, u32[]{:S(2)}, u32[]{:S(2)}) %collective-permute-start.15) | collective-permute-done | bytes 262176 | tf_op jit(solution)/shard_map/ppermute | solution.py:21
  311.8 2.3 fusion.25
  (301 shorter events, 99.8 us)
Async XLA Ops:
  6.5 33.0 %all-gather.21.cloned.1.call-start = ((), (), s32[]{:S(2)}) async-start(), calls=%async_computation.2 | async-start | bytes 1310720 | tf_op jit(solution)/shard_map/all_gather | solution.py:137
  8.5 59.8 %all-gather.17.cloned.1.call-start = ((), (), s32[]{:S(2)}) async-start(), calls=%async_computation | async-start | bytes 1310720 | tf_op jit(solution)/shard_map/all_gather | solution.py:142
  10.5 12.7 %copy-start.26 = (f32[4,513]{1,0:T(4,128)S(1)}, f32[4,513]{1,0:T(4,128)}, u32[]{:S(2)}) copy-start(f32[4,513]{1,0:T(4,128)} %param.21) | copy-start | bytes 24628
  10.5 12.9 %copy-start.25 = (f32[2,2048]{1,0:T(2,128)S(1)}, f32[2,2048]{1,0:T(2,128)}, u32[]{:S(2)}) copy-start(f32[2,2048]{1,0:T(2,128)} %param.14) | copy-start | bytes 49156
  10.5 13.0 %copy-start.2 = (bf16[256,2048]{1,0:T(8,128)(2,1)S(1)}, bf16[256,2048]{1,0:T(8,128)(2,1)}, u32[]{:S(2)}) copy-start(bf16[256,2048]{1,0:T(8,128)(2,1)} %param.12) | copy-start | bytes 3145732
  10.5 13.2 %copy-start.28 = (f32[2,64]{1,0:T(2,128)S(1)}, f32[2,64]{1,0:T(2,128)}, u32[]{:S(2)}) copy-start(f32[2,64]{1,0:T(2,128)} %param.19) | copy-start | bytes 1540
  10.5 13.2 %copy-start.29 = (f32[2,64]{1,0:T(2,128)S(1)}, f32[2,64]{1,0:T(2,128)}, u32[]{:S(2)}) copy-start(f32[2,64]{1,0:T(2,128)} %param.20) | copy-start | bytes 1540
  10.5 90.5 %all-gather.19.cloned.1.call-start = ((), (), s32[]{:S(2)}) async-start(), calls=%async_computation.1 | async-start | bytes 1310720 | tf_op jit(solution)/shard_map/all_gather | solution.py:132
  11.5 129.0 %all-gather.23.cloned.1.call-start = ((), (), s32[]{:S(2)}) async-start(), calls=%async_computation.3 | async-start | bytes 1310720 | tf_op jit(solution)/shard_map/all_gather | solution.py:167
  12.4 150.6 %all-gather.29.cloned.1.call-start = ((), (), s32[]{:S(2)}) async-start(), calls=%async_computation.6 | async-start | bytes 1310720 | tf_op jit(solution)/shard_map/all_gather | solution.py:137
  13.0 179.4 %all-gather.25.cloned.1.call-start = ((), (), s32[]{:S(2)}) async-start(), calls=%async_computation.4 | async-start | bytes 1310720 | tf_op jit(solution)/shard_map/all_gather | solution.py:142
  13.6 213.0 %all-gather.27.cloned.1.call-start = ((), (), s32[]{:S(2)}) async-start(), calls=%async_computation.5 | async-start | bytes 1310720 | tf_op jit(solution)/shard_map/all_gather | solution.py:132
  13.6 17.8 %collective-permute-start.1 = (s32[256]{0:T(256)S(1)}, s32[256]{0:T(256)S(1)}, u32[]{:S(2)}, u32[]{:S(2)}) collective-permute-start(s32[256]{0:T(256)S(1)} %copy-done.27), channel_id=1, source_target_pairs={{0,8},{4,12},{1,9},{5,13},{2,10},{6,14},{3,11},{7,15},{16,24},{20,... | collective-permute-start | bytes 3080 | tf_op jit(solution)/shard_map/ppermute | solution.py:35
  19.6 11.9 %collective-permute-start.2 = (s32[256]{0:T(256)S(1)}, s32[256]{0:T(256)S(1)}, u32[]{:S(2)}, u32[]{:S(2)}) collective-permute-start(s32[256]{0:T(256)S(1)} %copy-done.27), channel_id=1, source_target_pairs={{0,4},{4,8},{8,12},{1,5},{5,9},{9,13},{2,6},{6,10},{10,14},{3,7},{... | collective-permute-start | bytes 3080 | tf_op jit(solution)/shard_map/ppermute | solution.py:35
  23.1 269.6 %all-gather.31.cloned.1.call-start = ((), (), s32[]{:S(2)}) async-start(), calls=%async_computation.7 | async-start | bytes 1310720 | tf_op jit(solution)/shard_map/all_gather | solution.py:167
  31.4 90.2 %copy-start = (f32[4,64,576]{2,1,0:T(8,128)}, f32[4,64,576]{2,1,0:T(8,128)S(1)}, u32[]{:S(2)}) copy-start(f32[4,64,576]{2,1,0:T(8,128)S(1)} %copy.61) | copy-start | bytes 1769476
  31.9 89.7 %copy-start.3 = (pred[4,64,576]{2,1,0:T(8,128)(4,1)}, pred[4,64,576]{2,1,0:T(8,128)(4,1)S(1)}, u32[]{:S(2)}) copy-start(pred[4,64,576]{2,1,0:T(8,128)(4,1)S(1)} %compare_and_fusion) | copy-start | bytes 442372
  41.6 63.1 %collective-permute-start.3 = (bf16[256,256]{0,1:T(8,128)(2,1)S(1)}, bf16[256,256]{0,1:T(8,128)(2,1)S(1)}, u32[]{:S(2)}, u32[]{:S(2)}) collective-permute-start(bf16[256,256]{0,1:T(8,128)(2,1)S(1)} %fusion.76), channel_id=1, source_target_pairs={{0,8},{4,12},{1,9},{5,13},{2,10},{6,14},{3,11},{7,15},{16,24},{20,... | collective-permute-start | bytes 393224 | tf_op jit(solution)/shard_map/ppermute | solution.py:35
  45.4 60.5 %collective-permute-start.4 = (bf16[256,256]{0,1:T(8,128)(2,1)S(1)}, bf16[256,256]{0,1:T(8,128)(2,1)S(1)}, u32[]{:S(2)}, u32[]{:S(2)}) collective-permute-start(bf16[256,256]{0,1:T(8,128)(2,1)S(1)} %fusion.76), channel_id=1, source_target_pairs={{0,4},{4,8},{8,12},{1,5},{5,9},{9,13},{2,6},{6,10},{10,14},{3,7},{... | collective-permute-start | bytes 393224 | tf_op jit(solution)/shard_map/ppermute | solution.py:35
  70.1 44.7 %collective-permute-start.5 = (bf16[256,256]{1,0:T(8,128)(2,1)S(1)}, bf16[256,256]{1,0:T(8,128)(2,1)S(1)}, u32[]{:S(2)}, u32[]{:S(2)}) collective-permute-start(bf16[256,256]{1,0:T(8,128)(2,1)S(1)} %convolution_convert_fusion.1), channel_id=1, source_target_pairs={{0,4},{4,8},{8,12},{1,5},{5,9},{9,13},{2,6},{6,10},{10,14},{3,7},{... | collective-permute-start | bytes 393224 | tf_op jit(solution)/shard_map/ppermute | solution.py:35
  76.2 38.6 %collective-permute-start = (bf16[256,256]{1,0:T(8,128)(2,1)S(1)}, bf16[256,256]{1,0:T(8,128)(2,1)S(1)}, u32[]{:S(2)}, u32[]{:S(2)}) collective-permute-start(bf16[256,256]{1,0:T(8,128)(2,1)S(1)} %convolution_convert_fusion.1), channel_id=1, source_target_pairs={{0,8},{4,12},{1,9},{5,13},{2,10},{6,14},{3,11},{7,15},{16,24},{20,... | collective-permute-start | bytes 393224 | tf_op jit(solution)/shard_map/ppermute | solution.py:35
  142.3 5.8 %collective-permute-start.6 = (bf16[256,512]{1,0:T(8,128)(2,1)S(1)}, bf16[256,512]{1,0:T(8,128)(2,1)S(1)}, u32[]{:S(2)}, u32[]{:S(2)}) collective-permute-start(bf16[256,512]{1,0:T(8,128)(2,1)S(1)} %fusion.16), channel_id=1, source_target_pairs={{0,1},{1,2},{2,3},{3,0},{4,5},{5,6},{6,7},{7,4},{8,9},{9,10},{10,1... | collective-permute-start | bytes 786440 | tf_op jit(solution)/shard_map/ppermute | solution.py:21
  148.1 5.8 %collective-permute-start.7 = (bf16[256,512]{1,0:T(8,128)(2,1)S(1)}, bf16[256,512]{1,0:T(8,128)(2,1)S(1)}, u32[]{:S(2)}, u32[]{:S(2)}) collective-permute-start(bf16[256,512]{1,0:T(8,128)(2,1)S(1)} %collective-permute-done.6), channel_id=1, source_target_pairs={{0,1},{1,2},{2,3},{3,0},{4,5},{5,6},{6,7},{7,4},{8,9},{9,10},{10,1... | collective-permute-start | bytes 786440 | tf_op jit(solution)/shard_map/ppermute | solution.py:21
  153.9 5.8 %collective-permute-start.8 = (bf16[256,512]{1,0:T(8,128)(2,1)S(1)}, bf16[256,512]{1,0:T(8,128)(2,1)S(1)}, u32[]{:S(2)}, u32[]{:S(2)}) collective-permute-start(bf16[256,512]{1,0:T(8,128)(2,1)S(1)} %collective-permute-done.7), channel_id=1, source_target_pairs={{0,1},{1,2},{2,3},{3,0},{4,5},{5,6},{6,7},{7,4},{8,9},{9,10},{10,1... | collective-permute-start | bytes 786440 | tf_op jit(solution)/shard_map/ppermute | solution.py:21
  164.9 67.0 %collective-permute-start.10 = (bf16[256,256]{0,1:T(8,128)(2,1)S(1)}, bf16[256,256]{0,1:T(8,128)(2,1)}, u32[]{:S(2)}, u32[]{:S(2)}) collective-permute-start(bf16[256,256]{0,1:T(8,128)(2,1)S(1)} %fusion.74), channel_id=1, source_target_pairs={{0,8},{4,12},{1,9},{5,13},{2,10},{6,14},{3,11},{7,15},{16,24},{20,... | collective-permute-start | bytes 393224 | tf_op jit(solution)/shard_map/ppermute | solution.py:35
  170.7 64.2 %collective-permute-start.11 = (bf16[256,256]{0,1:T(8,128)(2,1)S(1)}, bf16[256,256]{0,1:T(8,128)(2,1)}, u32[]{:S(2)}, u32[]{:S(2)}) collective-permute-start(bf16[256,256]{0,1:T(8,128)(2,1)S(1)} %fusion.74), channel_id=1, source_target_pairs={{0,4},{4,8},{8,12},{1,5},{5,9},{9,13},{2,6},{6,10},{10,14},{3,7},{... | collective-permute-start | bytes 393224 | tf_op jit(solution)/shard_map/ppermute | solution.py:35
  194.7 63.9 %collective-permute-start.12 = (bf16[256,256]{1,0:T(8,128)(2,1)}, bf16[256,256]{1,0:T(8,128)(2,1)}, u32[]{:S(2)}, u32[]{:S(2)}) collective-permute-start(bf16[256,256]{1,0:T(8,128)(2,1)} %convolution_convert_fusion), channel_id=1, source_target_pairs={{0,4},{4,8},{8,12},{1,5},{5,9},{9,13},{2,6},{6,10},{10,14},{3,7},{... | collective-permute-start | bytes 393224 | tf_op jit(solution)/shard_map/ppermute | solution.py:35
  200.8 56.9 %collective-permute-start.9 = (bf16[256,256]{1,0:T(8,128)(2,1)}, bf16[256,256]{1,0:T(8,128)(2,1)}, u32[]{:S(2)}, u32[]{:S(2)}) collective-permute-start(bf16[256,256]{1,0:T(8,128)(2,1)} %convolution_convert_fusion), channel_id=1, source_target_pairs={{0,8},{4,12},{1,9},{5,13},{2,10},{6,14},{3,11},{7,15},{16,24},{20,... | collective-permute-start | bytes 393224 | tf_op jit(solution)/shard_map/ppermute | solution.py:35
  238.9 6.4 %copy-start.24 = (bf16[256,256]{0,1:T(8,128)(2,1)S(1)}, bf16[256,256]{0,1:T(8,128)(2,1)}, u32[]{:S(2)}) copy-start(bf16[256,256]{0,1:T(8,128)(2,1)} %get-tuple-element.23) | copy-start | bytes 393220
  294.4 5.8 %collective-permute-start.13 = (bf16[256,512]{1,0:T(8,128)(2,1)S(1)}, bf16[256,512]{1,0:T(8,128)(2,1)S(1)}, u32[]{:S(2)}, u32[]{:S(2)}) collective-permute-start(bf16[256,512]{1,0:T(8,128)(2,1)S(1)} %fusion.17), channel_id=1, source_target_pairs={{0,1},{1,2},{2,3},{3,0},{4,5},{5,6},{6,7},{7,4},{8,9},{9,10},{10,1... | collective-permute-start | bytes 786440 | tf_op jit(solution)/shard_map/ppermute | solution.py:21
  300.2 5.8 %collective-permute-start.14 = (bf16[256,512]{1,0:T(8,128)(2,1)S(1)}, bf16[256,512]{1,0:T(8,128)(2,1)S(1)}, u32[]{:S(2)}, u32[]{:S(2)}) collective-permute-start(bf16[256,512]{1,0:T(8,128)(2,1)S(1)} %collective-permute-done.13), channel_id=1, source_target_pairs={{0,1},{1,2},{2,3},{3,0},{4,5},{5,6},{6,7},{7,4},{8,9},{9,10},{10,1... | collective-permute-start | bytes 786440 | tf_op jit(solution)/shard_map/ppermute | solution.py:21
  306.0 5.8 %collective-permute-start.15 = (bf16[256,512]{1,0:T(8,128)(2,1)S(1)}, bf16[256,512]{1,0:T(8,128)(2,1)S(1)}, u32[]{:S(2)}, u32[]{:S(2)}) collective-permute-start(bf16[256,512]{1,0:T(8,128)(2,1)S(1)} %collective-permute-done.14), channel_id=1, source_target_pairs={{0,1},{1,2},{2,3},{3,0},{4,5},{5,6},{6,7},{7,4},{8,9},{9,10},{10,1... | collective-permute-start | bytes 786440 | tf_op jit(solution)/shard_map/ppermute | solution.py:21
  (22 other events, 56.1 us)
Sparse Core Ops, SparseCore 0:
  8.9 30.6 all-gather.20
  41.1 27.1 all-gather.16
  69.9 31.0 all-gather.18
  102.5 31.1 all-gather.22
  135.1 27.3 all-gather.28
  163.9 28.4 all-gather.24
  194.0 32.5 all-gather.26
  228.1 29.4 all-gather.30
